TPU v7x, 32 devices: a whole 2x2x4 slice. The times are simulated.
32 devices in a mesh: sp: 16 (over z, y, x), tp: 2 (over core).
Axes of the slice: x: 2, y: 2, z: 4, core: 2. Of those that a mesh axis runs over, the one named last changes fastest.
Arguments:
- resid: bfloat16 [3072, 2048], P(('sp', 'tp')), may hold values from -6 to 6
- queries: bfloat16 [3072, 2048], P('sp', 'tp'), may hold values from -8 to 8
- keys: bfloat16 [3072, 512], P('sp', 'tp'), may hold values from -8 to 8
- values: bfloat16 [3072, 512], P('sp', 'tp'), may hold values from -6 to 6
- log_gates: float32 [3072, 32], P('sp', 'tp'), may hold values from -1536 to 0, as said below
- out_gate: bfloat16 [3072, 2048], P('sp', 'tp'), may hold values from -8 to 8
- out_weight: bfloat16 [2048, 2048], P('tp'), may hold values from -0.125 to 0.125
- post_gain: float32 [2048], replicated, may hold values from 0.1 to 1.9
- pre_gain: float32 [2048], replicated, may hold values from 0.1 to 1.9
- ffn_gain: float32 [2048], replicated, may hold values from 0.1 to 1.9
- gate_weight: bfloat16 [2048, 5632], P('sp', 'tp'), may hold values from -0.125 to 0.125
- up_weight: bfloat16 [2048, 5632], P('sp', 'tp'), may hold values from -0.125 to 0.125
- down_weight: bfloat16 [5632, 2048], P('tp', 'sp'), may hold values from -0.078125 to 0.078125
Outputs:
- result: bfloat16 [3072, 2048], P(('sp', 'tp'))
Inputs may be any that keep to these rules, and one draw needn't show every extreme that they name: Each head's column of log_gates never rises from one position to the next, and its first entry is at most 0.
All inputs are finite; a program needn't handle non-finite values.
Results may differ from a plain program's by a relative error of at most 0.017.
Values may be sent and summed in bfloat16 or wider, within the bound.
A program may use at most 128 MiB of HBM per device.

v0:
```python
import jax
import jax.numpy as jnp
from jax import lax
from jax.sharding import PartitionSpec as P

HD = 64
EPS = 1e-06
KEY_BLOCK = 512


def rms_scale(rows, gain):
    mean_sq = jnp.mean(rows * rows, axis=-1, keepdims=True)
    return rows * lax.rsqrt(mean_sq + EPS) * gain


def shards(
    resid,
    queries,
    keys,
    values,
    log_gates,
    out_gate,
    out_weight,
    post_gain,
    pre_gain,
    ffn_gain,
    gate_weight,
    up_weight,
    down_weight,
):
    rows = queries.shape[0]
    head_size = HD
    kv_local = keys.shape[1] // head_size
    q_local = queries.shape[1] // head_size
    group = q_local // kv_local
    scale = head_size ** (-0.5)
    offset = lax.axis_index("sp") * rows
    last = offset + rows - 1
    query_pos = offset + jnp.arange(rows, dtype=jnp.int32)
    key_gates = lax.all_gather(log_gates, "sp", axis=0, tiled=True)
    query_blocks = queries.reshape(rows, kv_local, group, head_size)
    query_gates = log_gates.reshape(rows, kv_local, group).transpose(1, 2, 0)

    def key_block(carry, key_rows, value_rows, start):
        count = key_rows.shape[0]

        def compute(state):
            top, denom, accum = state
            scores = (
                jnp.einsum(
                    "tkgd,skd->kgts",
                    query_blocks,
                    key_rows.reshape(count, kv_local, head_size),
                    preferred_element_type=jnp.float32,
                )
                * scale
            )
            gates_here = (
                lax.dynamic_slice_in_dim(key_gates, start, count, 0)
                .reshape(count, kv_local, group)
                .transpose(1, 2, 0)
            )
            scores = scores + query_gates[:, :, :, None] - gates_here[:, :, None, :]
            causal = (start + jnp.arange(count, dtype=jnp.int32))[None, :] <= query_pos[:, None]
            scores = jnp.where(causal[None, None], scores, -jnp.inf)
            new_top = jnp.maximum(top, jnp.max(scores, axis=-1))
            shrink = jnp.exp(top - new_top)
            weights = jnp.exp(scores - new_top[..., None])
            denom = denom * shrink + jnp.sum(weights, axis=-1)
            accum = accum * shrink[..., None] + jnp.einsum(
                "kgts,skd->kgtd",
                weights.astype(jnp.bfloat16),
                value_rows.reshape(count, kv_local, head_size),
                preferred_element_type=jnp.float32,
            )
            return (new_top, denom, accum)

        def keep(state):
            return state

        return lax.cond(start <= last, compute, keep, carry)

    start_state = (
        jnp.full((kv_local, group, rows), -1e30, jnp.float32),
        jnp.zeros((kv_local, group, rows), jnp.float32),
        jnp.zeros((kv_local, group, rows, head_size), jnp.float32),
    )
    carry = start_state
    key_rows = lax.all_gather(keys, "sp", axis=0, tiled=True)
    value_rows = lax.all_gather(values, "sp", axis=0, tiled=True)
    count = key_rows.shape[0]
    blocks = count // KEY_BLOCK
    key_split = key_rows.reshape(blocks, KEY_BLOCK, key_rows.shape[1])
    value_split = value_rows.reshape(blocks, KEY_BLOCK, value_rows.shape[1])

    def advance(state, item):
        index, key_part, value_part = item
        return (key_block(state, key_part, value_part, index * KEY_BLOCK), None)

    carry, _ = lax.scan(
        advance, carry, (jnp.arange(blocks, dtype=jnp.int32), key_split, value_split)
    )
    top, denom, accum = carry
    attended = (accum / denom[..., None]).transpose(2, 0, 1, 3).reshape(rows, q_local * head_size)
    gated = (attended * jax.nn.sigmoid(out_gate.astype(jnp.float32))).astype(jnp.bfloat16)
    projected = lax.psum_scatter(
        jnp.dot(gated, out_weight, preferred_element_type=jnp.float32).astype(jnp.bfloat16),
        "tp",
        scatter_dimension=0,
        tiled=True,
    ).astype(jnp.float32)
    mixed = resid.astype(jnp.float32) + rms_scale(projected, post_gain)
    normed = rms_scale(mixed, pre_gain).astype(jnp.bfloat16)
    normed_all = lax.all_gather(normed, "tp", axis=0, tiled=True)
    gate = jnp.dot(
        normed_all,
        lax.all_gather(gate_weight, "sp", axis=0, tiled=True),
        preferred_element_type=jnp.float32,
    )
    up = jnp.dot(
        normed_all,
        lax.all_gather(up_weight, "sp", axis=0, tiled=True),
        preferred_element_type=jnp.float32,
    )
    hidden = (jax.nn.silu(gate) * up).astype(jnp.bfloat16)
    ffn_partial = jnp.dot(
        hidden,
        lax.all_gather(down_weight, "sp", axis=1, tiled=True),
        preferred_element_type=jnp.float32,
    )
    ffn = lax.psum_scatter(
        ffn_partial.astype(jnp.bfloat16), "tp", scatter_dimension=0, tiled=True
    ).astype(jnp.float32)
    return (mixed + rms_scale(ffn, ffn_gain)).astype(jnp.bfloat16)


def solution(mesh):
    in_specs = (
        P(("sp", "tp"), None),
        P("sp", "tp"),
        P("sp", "tp"),
        P("sp", "tp"),
        P("sp", "tp"),
        P("sp", "tp"),
        P("tp", None),
        P(),
        P(),
        P(),
        P("sp", "tp"),
        P("sp", "tp"),
        P("tp", "sp"),
    )
    out_specs = P(("sp", "tp"), None)
    return jax.shard_map(shards, mesh=mesh, in_specs=in_specs, out_specs=out_specs, check_vma=False)
```

profile of v0, /device:TPU:0, one launch (start us, length us, event | category | flops | bytes accessed | tf_op | source)
XLA Modules:
  0.0 712.2 jit_solution(13522817512439941888)
XLA Ops:
  6.5 0.7 all-gather.7.cloned.1.call-update
  7.3 0.7 all-gather.9.cloned.1.call-update
  8.0 0.0 reduce-scatter.3.cloned.1.call-start
  8.1 0.7 reshape.101
  8.8 44.2 %all-gather = f32[16,192,16]{1,2,0:T(8,128)S(1)} all-gather(f32[1,192,16]{1,2,0:T(8,128)} %bitcast.74), channel_id=1, replica_groups=mesh['sp'=16,'tp'=2] {'sp'}, dimensions={0}, use_global_device_ids=true | all-gather | bytes 208896 | tf_op jit(solution)/shard_map/all_gather | solution.py:40
  52.9 0.2 copy.27
  53.1 0.1 reshape.105
  53.2 2.0 copy.26
  55.2 15.7 %all-gather.7.cloned.1.call-done = bf16[3072,256]{1,0:T(8,128)(2,1)} async-done(((bf16[192,256]{1,0:T(8,128)(2,1)}), bf16[3072,256]{1,0:T(8,128)(2,1)}) %all-gather.7.cloned.1.call-update) | async-done | bytes 1572880 | tf_op jit(solution)/shard_map/all_gather | solution.py:89
  70.9 1.7 copy.28
  72.7 57.8 %all-gather.9.cloned.1.call-done = bf16[3072,256]{1,0:T(8,128)(2,1)} async-done(((bf16[192,256]{1,0:T(8,128)(2,1)}), bf16[3072,256]{1,0:T(8,128)(2,1)}) %all-gather.9.cloned.1.call-update) | async-done | bytes 1572880 | tf_op jit(solution)/shard_map/all_gather | solution.py:90
  130.4 1.7 copy.29
  132.2 1.1 broadcast_in_dim.42
  133.3 17.4 %while.15 = (s32[]{:T(128)}, f32[4,4,192]{2,1,0:T(4,128)S(1)}, f32[4,4,192]{2,1,0:T(4,128)S(1)}, f32[4,4,192,64]{2,3,1,0:T(8,128)}, s32[6]{0:T(128)S(1)}, /*inde...) while((s32[]{:T(128)}, f32[4,4,192]{2,1,0:T(4,128)S(1)}, ...), condition=%wide.region_5.6_spmd.clone, body=%wide.region_0.5_spmd.clone.sunk | while | flops 429890240 | bytes 29568428 | solution.py:100
  133.3 0.6 dynamic_slice.31
  134.5 9.6 %conditional.3 = ((f32[4,4,192]{2,1,0:T(4,128)S(1)}, f32[4,4,192]{2,1,0:T(4,128)S(1)}, f32[4,4,192,64]{2,3,1,0:T(8,128)})) conditional(s32[]{:T(128)} %convert_element_type.96, (f32[4,4,192]{2,1,0:T(4,128)S(1)}, f32[4,4,192]{2,1,0:T(4,128)S(1)}, f32[4,4,192,64]{2,3,1,0:T(8,128)}) %tuple.43, (s32[]{:T(128)}, s32[]{:T(128)}, ...), branch_computations={%region_1.1_spmd, %region_2.4_spmd} | conditional | flops 429890240 | bytes 29567370 | solution.py:81
  134.5 0.1 constant_dynamic-slice_fusion.1
  134.7 0.1 broadcast_compare_fusion
  134.9 3.4 fusion.6
  138.2 2.5 fusion.5
  140.8 2.3 fusion.10
  143.1 1.0 copy-done.2
  144.1 0.6 dynamic_slice.31
  145.4 0.6 dynamic_slice.31
  146.7 0.6 dynamic_slice.31
  148.0 0.6 dynamic_slice.31
  149.3 0.6 dynamic_slice.31
  150.6 1.3 broadcast_divide_fusion
  152.0 0.3 copy.30
  152.3 4.3 convolution_convert_fusion.1
  156.6 0.0 all-gather.11.cloned.1.call-start
  156.7 0.5 all-gather.11.cloned.1.call-update
  157.3 0.5 all-gather.13.cloned.1.call-update
  157.8 0.5 all-gather.15.cloned.1.call-update
  158.4 0.0 reduce-scatter.5.cloned.1.call-start
  158.4 53.0 %reduce-scatter.3.cloned.1.call-done = bf16[96,2048]{1,0:T(8,128)(2,1)} async-done(((bf16[192,2048]{1,0:T(8,128)(2,1)}), bf16[96,2048]{1,0:T(8,128)(2,1)}) %reduce-scatter.3.cloned.1.call-update) | async-done | bytes 393232 | tf_op jit(solution)/shard_map/reduce_scatter | solution.py:106
  211.4 1.2 fusion.16
  212.6 1.3 multiply_reduce_fusion
  214.0 1.3 multiply_convert_fusion
  215.3 2.5 all_gather.24
  217.8 138.8 %all-gather.11.cloned.1.call-done = bf16[2048,2816]{1,0:T(8,128)(2,1)} async-done(((bf16[128,2816]{1,0:T(8,128)(2,1)}), bf16[2048,2816]{1,0:T(8,128)(2,1)}) %all-gather.11.cloned.1.call-update) | async-done | bytes 11534352 | tf_op jit(solution)/shard_map/all_gather | solution.py:117
  356.6 8.0 %fusion.26 = f32[192,2816]{1,0:T(8,128)} fusion(bf16[192,2048]{1,0:T(8,128)(2,1)S(1)} %all_gather.24, bf16[2048,2816]{1,0:T(8,128)(2,1)} %all-gather.11.cloned.1.call-done), kind=kOutput, calls=%fused_computation.46 | convolution fusion | flops 2214592512 | bytes 14483456 | tf_op jit(solution)/shard_map/dot_general | solution.py:115
  364.6 134.2 %all-gather.13.cloned.1.call-done = bf16[2048,2816]{1,0:T(8,128)(2,1)} async-done(((bf16[128,2816]{1,0:T(8,128)(2,1)}), bf16[2048,2816]{1,0:T(8,128)(2,1)}) %all-gather.13.cloned.1.call-update) | async-done | bytes 11534352 | tf_op jit(solution)/shard_map/all_gather | solution.py:122
  498.8 182.8 %all-gather.15.cloned.1.call-done = bf16[2816,2048]{1,0:T(8,128)(2,1)} async-done(((bf16[2816,128]{1,0:T(8,128)(2,1)}), bf16[2816,2048]{1,0:T(8,128)(2,1)}) %all-gather.15.cloned.1.call-update) | async-done | bytes 11534352 | tf_op jit(solution)/shard_map/all_gather | solution.py:128
  681.6 13.9 %convolution_convert_fusion = bf16[192,2048]{1,0:T(8,128)(2,1)} fusion(bf16[2816,2048]{1,0:T(8,128)(2,1)} %all-gather.15.cloned.1.call-done, bf16[192,2048]{1,0:T(8,128)(2,1)S(1)} %all_gather.24, bf16[2048,2816]{1,0:T(8,128)(2,1)} %all-gather.13.cloned.1.call-done, f32[192,2816]{1,0:T(8,128)} %fusion.26), kind=kOutput, calls=%fused_computation.23 | convolution fusion | flops 4432822272 | bytes 26804224 | tf_op jit(solution)/shard_map/dot_general | solution.py:126
  695.5 6.5 reduce-scatter.5.cloned.1.call-done
  702.0 1.2 fusion.19
  703.2 2.1 fusion.22
  (43 shorter events, 0.4 us)
Async XLA Ops:
  6.5 64.4 %all-gather.7.cloned.1.call-start = ((), (), s32[]{:S(2)}) async-start(), calls=%async_computation.2 | async-start | bytes 1671168 | tf_op jit(solution)/shard_map/all_gather | solution.py:89
  7.3 123.2 %all-gather.9.cloned.1.call-start = ((), (), s32[]{:S(2)}) async-start(), calls=%async_computation.3 | async-start | bytes 1671168 | tf_op jit(solution)/shard_map/all_gather | solution.py:90
  8.0 203.4 %reduce-scatter.3.cloned.1.call-start = ((), (), s32[]{:S(2)}) async-start(), calls=%async_computation.4 | async-start | bytes 1179648 | tf_op jit(solution)/shard_map/reduce_scatter | solution.py:106
  134.8 6.0 copy-start.1
  143.1 1.0 copy-start.2
  152.3 60.3 %copy-start.3 = (bf16[96,2048]{1,0:T(8,128)(2,1)S(1)}, bf16[96,2048]{1,0:T(8,128)(2,1)}, u32[]{:S(2)}) copy-start(bf16[96,2048]{1,0:T(8,128)(2,1)} %param.17) | copy-start | bytes 1179652
  152.3 60.3 %copy-start.4 = (f32[2048]{0:T(1024)S(1)}, f32[2048]{0:T(1024)}, u32[]{:S(2)}) copy-start(f32[2048]{0:T(1024)} %param.24) | copy-start | bytes 24580
  152.3 61.7 %copy-start.5 = (f32[2048]{0:T(1024)S(1)}, f32[2048]{0:T(1024)}, u32[]{:S(2)}) copy-start(f32[2048]{0:T(1024)} %param.25) | copy-start | bytes 24580
  156.6 200.0 %all-gather.11.cloned.1.call-start = ((), (), s32[]{:S(2)}) async-start(), calls=%async_computation.5 | async-start | bytes 12255232 | tf_op jit(solution)/shard_map/all_gather | solution.py:117
  157.2 341.6 %all-gather.13.cloned.1.call-start = ((), (), s32[]{:S(2)}) async-start(), calls=%async_computation.6 | async-start | bytes 12255232 | tf_op jit(solution)/shard_map/all_gather | solution.py:122
  157.8 523.8 %all-gather.15.cloned.1.call-start = ((), (), s32[]{:S(2)}) async-start(), calls=%async_computation.7 | async-start | bytes 12255232 | tf_op jit(solution)/shard_map/all_gather | solution.py:128
  158.4 543.6 %reduce-scatter.5.cloned.1.call-start = ((), (), s32[]{:S(2)}) async-start(), calls=%async_computation.8 | async-start | bytes 1179648 | tf_op jit(solution)/shard_map/reduce_scatter | solution.py:131
  364.6 338.6 %copy-start = (bf16[96,2048]{1,0:T(8,128)(2,1)S(1)}, bf16[96,2048]{1,0:T(8,128)(2,1)}, u32[]{:S(2)}) copy-start(bf16[96,2048]{1,0:T(8,128)(2,1)} %reduce-scatter.3.cloned.1.call-done) | copy-start | bytes 1179652
  364.6 338.6 %copy-start.6 = (f32[2048]{0:T(1024)S(1)}, f32[2048]{0:T(1024)}, u32[]{:S(2)}) copy-start(f32[2048]{0:T(1024)} %param.26) | copy-start | bytes 24580
Sparse Core Ops, SparseCore 0:
  10.1 60.7 all-gather.6
  73.7 56.6 all-gather.8
  156.8 54.6 reduce-scatter.2
  214.0 142.5 all-gather.10
  359.2 139.5 all-gather.12
  501.4 180.2 all-gather.14
  695.6 6.3 reduce-scatter.4
where the time goes:
time: 713 us; the launch traced here: 712 us
  waiting for transfers between devices  592 us (83%)
  blocking collectives  46.7 us (7%)
  matrix products  31.8 us (4%)
  between operations  13.6 us (2%)
  local copies, waits for them, and re-layouts  12.7 us (2%)
  other arithmetic  11.1 us (2%)
    all_gather x1, waiting for transfers between devices, shards(): lax.all_gather(down_weight, 'sp', axis=1, tiled=True)  183 us
    all_gather x1, waiting for transfers between devices, shards(): lax.all_gather(gate_weight, 'sp', axis=0, tiled=True)  139 us
    all_gather x1, waiting for transfers between devices, shards(): lax.all_gather(up_weight, 'sp', axis=0, tiled=True)  134 us
    all_gather x1, waiting for transfers between devices, shards(): value_rows = lax.all_gather(values, 'sp', axis=0, tiled=True)  57.8 us
    reduce_scatter x1, waiting for transfers between devices, shards(): lax.psum_scatter(jnp.dot(gated, out_weight, preferred_element_type=jnp.fl...  53 us
    all_gather x1, blocking collectives, shards(): key_gates = lax.all_gather(log_gates, 'sp', axis=0, tiled=True)  44.2 us
    all_gather x1, waiting for transfers between devices, shards(): key_rows = lax.all_gather(keys, 'sp', axis=0, tiled=True)  15.7 us
  transfers between devices with their start and end apart: 7, of which 7 were waited for; matrix products, arithmetic and copies ran while one was open for 2% of the time, Pallas kernels for 0%

commit v1 on v0

--- a/solution.py
+++ b/solution.py
@@ -6,6 +6,20 @@
 HD = 64
 EPS = 1e-06
 KEY_BLOCK = 512
+
+
+def record_map(u_in):
+    taken_in, part_next, w_next = (lax.axis_size("sp"), lax.axis_index("sp"), u_in.shape[1])
+    y1, outer = (u_in, 1)
+    while outer < taken_in:
+        slots = []
+        ix = 0
+        while ix < taken_in:
+            slots.append((ix, (ix - outer) % taken_in))
+            ix += 1
+        y1 = jnp.concatenate([y1, lax.ppermute(y1, "sp", slots)], 1)
+        outer = 2 * outer
+    return jnp.roll(y1, part_next * w_next, 1)
 
 
 def rms_scale(rows, gain):
@@ -123,11 +137,7 @@
         preferred_element_type=jnp.float32,
     )
     hidden = (jax.nn.silu(gate) * up).astype(jnp.bfloat16)
-    ffn_partial = jnp.dot(
-        hidden,
-        lax.all_gather(down_weight, "sp", axis=1, tiled=True),
-        preferred_element_type=jnp.float32,
-    )
+    ffn_partial = jnp.dot(hidden, record_map(down_weight), preferred_element_type=jnp.float32)
     ffn = lax.psum_scatter(
         ffn_partial.astype(jnp.bfloat16), "tp", scatter_dimension=0, tiled=True
     ).astype(jnp.float32)

time: 713 us -> 843 us (1.18)
  starting transfers between devices: 0.23 us -> 53.2 us
  waiting for transfers between devices: 592 us -> 637 us
  local copies, waits for them, and re-layouts: 12.7 us -> 39 us
    ppermute x0 -> x4, waiting for transfers between devices: none -> 460 us  [record_map(): y1 = jnp.concatenate([y1, lax.ppermute(y1, 'sp', slots)], 1)]
    all_gather x1 -> x0, waiting for transfers between devices: 183 us -> none  [shards(): lax.all_gather(down_weight, 'sp', axis=1, tiled=True)]
    all_gather x1, waiting for transfers between devices: 139 us -> 0.01 us  [shards(): lax.all_gather(gate_weight, 'sp', axis=0, tiled=True)]
    reduce_scatter x1, waiting for transfers between devices: 53 us -> 0.01 us  [shards(): lax.psum_scatter(jnp.dot(gated, out_weight, preferred_element_type=jnp.fl...]
    ppermute x0 -> x4, starting transfers between devices: none -> 53 us  [record_map(): y1 = jnp.concatenate([y1, lax.ppermute(y1, 'sp', slots)], 1)]
    all_gather x1, waiting for transfers between devices: 134 us -> 94.9 us  [shards(): lax.all_gather(up_weight, 'sp', axis=0, tiled=True)]
    unnamed x14 -> x37, local copies, waits for them, and re-layouts: 5.59 us -> 25.2 us
  transfers between devices with their start and end apart: 7 -> 10, of which waited for: 7 -> 8; matrix products, arithmetic and copies ran while one was open for 2% -> 6% of each run, Pallas kernels for 0% -> 0%
where the time goes in v1:
time: 843 us; the launch traced here: 842 us
  waiting for transfers between devices  637 us (76%)
  starting transfers between devices  53.2 us (6%)
  blocking collectives  47.4 us (6%)
  local copies, waits for them, and re-layouts  39 us (5%)
  matrix products  31.9 us (4%)
  other arithmetic  15.6 us (2%)
  between operations  13.7 us (2%)
    ppermute x4, waiting for transfers between devices, record_map(): y1 = jnp.concatenate([y1, lax.ppermute(y1, 'sp', slots)], 1)  460 us
    all_gather x1, waiting for transfers between devices, shards(): lax.all_gather(up_weight, 'sp', axis=0, tiled=True)  94.9 us
    all_gather x1, waiting for transfers between devices, shards(): value_rows = lax.all_gather(values, 'sp', axis=0, tiled=True)  57.8 us
    ppermute x4, starting transfers between devices, record_map(): y1 = jnp.concatenate([y1, lax.ppermute(y1, 'sp', slots)], 1)  53 us
    all_gather x1, blocking collectives, shards(): key_gates = lax.all_gather(log_gates, 'sp', axis=0, tiled=True)  44.7 us
    unnamed x37, local copies, waits for them, and re-layouts  25.2 us
  transfers between devices with their start and end apart: 10, of which 8 were waited for; matrix products, arithmetic and copies ran while one was open for 6% of the time, Pallas kernels for 0%

profile of v1, /device:TPU:0, one launch (start us, length us, event | category | flops | bytes accessed | tf_op | source)
XLA Modules:
  0.0 842.0 jit_solution(17524650583719050473)
XLA Ops:
  6.5 0.7 all-gather.6.cloned.1.call-update
  7.3 0.7 all-gather.8.cloned.1.call-update
  8.1 2.0 copy.26
  10.1 0.7 reshape.101
  10.8 44.7 %all-gather = f32[16,192,16]{1,2,0:T(8,128)S(1)} all-gather(f32[1,192,16]{1,2,0:T(8,128)} %bitcast.73), channel_id=1, replica_groups=mesh['sp'=16,'tp'=2] {'sp'}, dimensions={0}, use_global_device_ids=true | all-gather | bytes 208896 | tf_op jit(solution)/shard_map/all_gather | solution.py:54
  55.8 15.2 %all-gather.6.cloned.1.call-done = bf16[3072,256]{1,0:T(8,128)(2,1)} async-done(((bf16[192,256]{1,0:T(8,128)(2,1)}), bf16[3072,256]{1,0:T(8,128)(2,1)}) %all-gather.6.cloned.1.call-update) | async-done | bytes 1572880 | tf_op jit(solution)/shard_map/all_gather | solution.py:103
  71.0 1.7 copy.28
  72.7 57.8 %all-gather.8.cloned.1.call-done = bf16[3072,256]{1,0:T(8,128)(2,1)} async-done(((bf16[192,256]{1,0:T(8,128)(2,1)}), bf16[3072,256]{1,0:T(8,128)(2,1)}) %all-gather.8.cloned.1.call-update) | async-done | bytes 1572880 | tf_op jit(solution)/shard_map/all_gather | solution.py:104
  130.5 1.7 copy.29
  132.2 1.1 broadcast_in_dim.42
  133.3 17.7 %while.15 = (s32[]{:T(128)}, f32[4,4,192]{2,1,0:T(4,128)S(1)}, f32[4,4,192]{2,1,0:T(4,128)S(1)}, f32[4,4,192,64]{2,3,1,0:T(8,128)}, s32[6]{0:T(128)S(1)}, /*inde...) while((s32[]{:T(128)}, f32[4,4,192]{2,1,0:T(4,128)S(1)}, ...), condition=%wide.region_5.6_spmd.clone, body=%wide.region_0.5_spmd.clone.sunk | while | flops 429890240 | bytes 29568436 | solution.py:114
  134.6 9.6 %conditional.3 = ((f32[4,4,192]{2,1,0:T(4,128)S(1)}, f32[4,4,192]{2,1,0:T(4,128)S(1)}, f32[4,4,192,64]{2,3,1,0:T(8,128)})) conditional(s32[]{:T(128)} %convert_element_type.96, (f32[4,4,192]{2,1,0:T(4,128)S(1)}, f32[4,4,192]{2,1,0:T(4,128)S(1)}, f32[4,4,192,64]{2,3,1,0:T(8,128)}) %tuple.43, (s32[]{:T(128)}, s32[]{:T(128)}, ...), branch_computations={%region_1.1_spmd, %region_2.4_spmd} | conditional | flops 429890240 | bytes 29567370 | solution.py:95
  135.0 3.4 fusion.6
  138.4 2.5 fusion.5
  140.9 2.3 fusion.10
  143.3 1.0 copy-done.8
  145.6 0.7 dynamic_slice.40
  147.0 0.7 dynamic_slice.40
  149.6 0.7 dynamic_slice.40
  151.0 1.3 broadcast_divide_fusion
  152.7 4.2 convolution_convert_fusion
  158.1 50.9 %collective-permute-start = (bf16[2816,128]{1,0:T(8,128)(2,1)S(1)}, bf16[2816,128]{1,0:T(8,128)(2,1)S(1)}, u32[]{:S(2)}, u32[]{:S(2)}) collective-permute-start(bf16[2816,128]{1,0:T(8,128)(2,1)S(1)} %copy-done.2), channel_id=1, source_target_pairs={{0,30},{2,0},{4,2},{6,4},{8,6},{10,8},{12,10},{14,12},{16,14},{18,... | collective-permute-start | bytes 2162696 | tf_op jit(solution)/shard_map/ppermute | solution.py:20
  209.0 14.0 %collective-permute-done = bf16[2816,128]{1,0:T(8,128)(2,1)S(1)} collective-permute-done((bf16[2816,128]{1,0:T(8,128)(2,1)S(1)}, bf16[2816,128]{1,0:T(8,128)(2,1)S(1)}, u32[]{:S(2)}, u32[]{:S(2)}) %collective-permute-start) | collective-permute-done | bytes 720928 | tf_op jit(solution)/shard_map/ppermute | solution.py:20
  223.2 1.9 collective-permute-start.1
  225.1 45.9 %collective-permute-done.1 = bf16[2816,256]{1,0:T(8,128)(2,1)S(1)} collective-permute-done((bf16[2816,256]{1,0:T(8,128)(2,1)S(1)}, bf16[2816,256]{1,0:T(8,128)(2,1)S(1)}, u32[]{:S(2)}, u32[]{:S(2)}) %collective-permute-start.1) | collective-permute-done | bytes 1441824 | tf_op jit(solution)/shard_map/ppermute | solution.py:20
  271.3 59.4 %collective-permute-done.2 = bf16[2816,512]{1,0:T(8,128)(2,1)S(1)} collective-permute-done((bf16[2816,512]{1,0:T(8,128)(2,1)S(1)}, bf16[2816,512]{1,0:T(8,128)(2,1)S(1)}, u32[]{:S(2)}, u32[]{:S(2)}) %collective-permute-start.2) | collective-permute-done | bytes 2883616 | tf_op jit(solution)/shard_map/ppermute | solution.py:20
  330.8 4.1 pad_maximum_fusion
  335.0 2.1 constant_dynamic-update-slice_fusion.9
  337.1 2.1 constant_dynamic-update-slice_fusion.8
  339.1 2.8 constant_dynamic-update-slice_fusion.7
  342.0 1.2 fusion.21
  343.2 1.3 multiply_reduce_fusion
  344.6 1.3 multiply_convert_fusion
  345.8 2.7 all_gather.21
  348.5 1.9 constant_dynamic-update-slice_fusion.6
  350.4 340.8 %collective-permute-done.3 = bf16[2816,1024]{1,0:T(8,128)(2,1)} collective-permute-done((bf16[2816,1024]{1,0:T(8,128)(2,1)}, bf16[2816,1024]{1,0:T(8,128)(2,1)}, u32[]{:S(2)}, u32[]{:S(2)}) %collective-permute-start.3) | collective-permute-done | bytes 5767200 | tf_op jit(solution)/shard_map/ppermute | solution.py:20
  691.2 5.7 constant_dynamic-update-slice_fusion.5
  696.9 0.9 constant_dynamic-update-slice_fusion.4
  697.9 1.0 constant_dynamic-update-slice_fusion.3
  698.8 1.2 constant_dynamic-update-slice_fusion.2
  700.1 1.8 constant_dynamic-update-slice_fusion.1
  701.9 6.4 constant_dynamic-update-slice_fusion
  708.3 8.1 fusion.32
  716.4 94.9 %all-gather.12.cloned.1.call-done = bf16[2048,2816]{1,0:T(8,128)(2,1)} async-done(((bf16[128,2816]{1,0:T(8,128)(2,1)}), bf16[2048,2816]{1,0:T(8,128)(2,1)}) %all-gather.12.cloned.1.call-update) | async-done | bytes 11534352 | tf_op jit(solution)/shard_map/all_gather | solution.py:136
  811.3 13.9 %fusion.18 = bf16[192,2048]{1,0:T(8,128)(2,1)} fusion(bf16[2816,4096]{1,0:T(8,128)(2,1)} %constant_dynamic-update-slice_fusion, s32[]{:T(128)S(6)} %select_n.25, bf16[192,2048]{1,0:T(8,128)(2,1)S(1)} %copy-done.10, bf16[2048,2816]{1,0:T(8,128)(2,1)} %all-gather.12.cloned.1.call-done, f32[192,2816]{1,0:T(8,128)} %fusion.32), kind=kOutput, calls=%fused_computation.27 | convolution fusion | flops 4432822272 | bytes 26804228 | tf_op jit(solution)/shard_map/dot_general | solution.py:140
  825.2 6.6 reduce-scatter.5.cloned.1.call-done
  831.8 1.2 fusion.24
  833.0 2.1 fusion.27
  (75 shorter events, 4.8 us)
Async XLA Ops:
  6.5 64.5 %all-gather.6.cloned.1.call-start = ((), (), s32[]{:S(2)}) async-start(), calls=%async_computation.2 | async-start | bytes 1671168 | tf_op jit(solution)/shard_map/all_gather | solution.py:103
  7.3 123.2 %all-gather.8.cloned.1.call-start = ((), (), s32[]{:S(2)}) async-start(), calls=%async_computation.3 | async-start | bytes 1671168 | tf_op jit(solution)/shard_map/all_gather | solution.py:104
  8.0 334.0 %reduce-scatter.3.cloned.1.call-start = ((), (), s32[]{:S(2)}) async-start(), calls=%async_computation.4 | async-start | bytes 1179648 | tf_op jit(solution)/shard_map/reduce_scatter | solution.py:120
  135.0 6.0 copy-start.7
  143.3 1.0 copy-start.8
  152.3 5.8 copy-start.2
  156.9 551.4 %all-gather.10.cloned.1.call-start = ((), (), s32[]{:S(2)}) async-start(), calls=%async_computation.5 | async-start | bytes 12255232 | tf_op jit(solution)/shard_map/all_gather | solution.py:131
  157.5 653.8 %all-gather.12.cloned.1.call-start = ((), (), s32[]{:S(2)}) async-start(), calls=%async_computation.6 | async-start | bytes 12255232 | tf_op jit(solution)/shard_map/all_gather | solution.py:136
  158.1 673.7 %reduce-scatter.5.cloned.1.call-start = ((), (), s32[]{:S(2)}) async-start(), calls=%async_computation.7 | async-start | bytes 1179648 | tf_op jit(solution)/shard_map/reduce_scatter | solution.py:141
  158.1 64.9 %collective-permute-start = (bf16[2816,128]{1,0:T(8,128)(2,1)S(1)}, bf16[2816,128]{1,0:T(8,128)(2,1)S(1)}, u32[]{:S(2)}, u32[]{:S(2)}) collective-permute-start(bf16[2816,128]{1,0:T(8,128)(2,1)S(1)} %copy-done.2), channel_id=1, source_target_pairs={{0,30},{2,0},{4,2},{6,4},{8,6},{10,8},{12,10},{14,12},{16,14},{18,... | collective-permute-start | bytes 2162696 | tf_op jit(solution)/shard_map/ppermute | solution.py:20
  223.0 111.9 %copy-start.4 = (bf16[2816,128]{1,0:T(8,128)(2,1)}, bf16[2816,128]{1,0:T(8,128)(2,1)S(1)}, u32[]{:S(2)}) copy-start(bf16[2816,128]{1,0:T(8,128)(2,1)S(1)} %collective-permute-done) | copy-start | bytes 2162692
  223.2 47.8 %collective-permute-start.1 = (bf16[2816,256]{1,0:T(8,128)(2,1)S(1)}, bf16[2816,256]{1,0:T(8,128)(2,1)S(1)}, u32[]{:S(2)}, u32[]{:S(2)}) collective-permute-start(bf16[2816,256]{1,0:T(8,128)(2,1)S(1)} %pad_maximum_fusion.2), channel_id=1, source_target_pairs={{0,28},{2,30},{4,0},{6,2},{8,4},{10,6},{12,8},{14,10},{16,12},{18,... | collective-permute-start | bytes 4325384 | tf_op jit(solution)/shard_map/ppermute | solution.py:20
  271.0 63.9 %copy-start = (bf16[2816,256]{1,0:T(8,128)(2,1)}, bf16[2816,256]{1,0:T(8,128)(2,1)S(1)}, u32[]{:S(2)}) copy-start(bf16[2816,256]{1,0:T(8,128)(2,1)S(1)} %collective-permute-done.1) | copy-start | bytes 4325380
  271.3 71.9 %copy-start.9 = (bf16[96,2048]{1,0:T(8,128)(2,1)S(1)}, bf16[96,2048]{1,0:T(8,128)(2,1)}, u32[]{:S(2)}) copy-start(bf16[96,2048]{1,0:T(8,128)(2,1)} %param.17) | copy-start | bytes 1179652
  271.3 71.9 %copy-start.11 = (f32[2048]{0:T(1024)S(1)}, f32[2048]{0:T(1024)}, u32[]{:S(2)}) copy-start(f32[2048]{0:T(1024)} %param.24) | copy-start | bytes 24580
  271.3 59.5 %collective-permute-start.2 = (bf16[2816,512]{1,0:T(8,128)(2,1)S(1)}, bf16[2816,512]{1,0:T(8,128)(2,1)S(1)}, u32[]{:S(2)}, u32[]{:S(2)}) collective-permute-start(bf16[2816,512]{1,0:T(8,128)(2,1)S(1)} %pad_maximum_fusion.1), channel_id=1, source_target_pairs={{0,24},{2,26},{4,28},{6,30},{8,0},{10,2},{12,4},{14,6},{16,8},{18,... | collective-permute-start | bytes 8650760 | tf_op jit(solution)/shard_map/ppermute | solution.py:20
  334.9 9.7 %copy-start.12 = (f32[2048]{0:T(1024)S(1)}, f32[2048]{0:T(1024)}, u32[]{:S(2)}) copy-start(f32[2048]{0:T(1024)} %param.25) | copy-start | bytes 24580
  334.9 356.3 %collective-permute-start.3 = (bf16[2816,1024]{1,0:T(8,128)(2,1)}, bf16[2816,1024]{1,0:T(8,128)(2,1)}, u32[]{:S(2)}, u32[]{:S(2)}) collective-permute-start(bf16[2816,1024]{1,0:T(8,128)(2,1)} %pad_maximum_fusion), channel_id=1, source_target_pairs={{0,16},{2,18},{4,20},{6,22},{8,24},{10,26},{12,28},{14,30},{16,0},... | collective-permute-start | bytes 17301512 | tf_op jit(solution)/shard_map/ppermute | solution.py:20
  350.4 346.5 %copy-start.3 = (bf16[2816,128]{1,0:T(8,128)(2,1)S(1)}, bf16[2816,128]{1,0:T(8,128)(2,1)}, u32[]{:S(2)}) copy-start(bf16[2816,128]{1,0:T(8,128)(2,1)} %param.29) | copy-start | bytes 2162692
  350.4 347.5 %copy-start.5 = (bf16[2816,128]{1,0:T(8,128)(2,1)S(1)}, bf16[2816,128]{1,0:T(8,128)(2,1)}, u32[]{:S(2)}) copy-start(bf16[2816,128]{1,0:T(8,128)(2,1)} %copy-done.4) | copy-start | bytes 2162692
  350.4 348.4 %copy-start.1 = (bf16[2816,256]{1,0:T(8,128)(2,1)S(1)}, bf16[2816,256]{1,0:T(8,128)(2,1)}, u32[]{:S(2)}) copy-start(bf16[2816,256]{1,0:T(8,128)(2,1)} %copy-done) | copy-start | bytes 4325380
  701.9 6.4 copy-start.10
  716.4 116.6 %copy-start.6 = (bf16[96,2048]{1,0:T(8,128)(2,1)S(1)}, bf16[96,2048]{1,0:T(8,128)(2,1)}, u32[]{:S(2)}) copy-start(bf16[96,2048]{1,0:T(8,128)(2,1)} %reduce-scatter.3.cloned.1.call-done) | copy-start | bytes 1179652
  716.4 116.6 %copy-start.13 = (f32[2048]{0:T(1024)S(1)}, f32[2048]{0:T(1024)}, u32[]{:S(2)}) copy-start(f32[2048]{0:T(1024)} %param.26) | copy-start | bytes 24580
Sparse Core Ops, SparseCore 0:
  10.1 60.8 all-gather.5
  73.8 56.6 all-gather.7
  157.0 54.7 reduce-scatter.2
  214.4 399.3 all-gather.9
  616.4 194.7 all-gather.11
  825.3 6.4 reduce-scatter.4
